TPU v7x, 256 devices: a whole 4x4x8 slice. The times are simulated.
256 devices in a mesh: sp: 32 (over z, x), tp: 8 (over y, core).
Axes of the slice: x: 4, y: 4, z: 8, core: 2. Of those that a mesh axis runs over, the one named last changes fastest.
Arguments:
- tokens: bfloat16 [32768, 2048], P('sp', 'tp'), may hold values from -70 to 70
- w_query: bfloat16 [2048, 1024], P(None, 'tp'), may hold values from -0.125 to 0.125
- w_key: bfloat16 [2048, 1024], P(None, 'tp'), may hold values from -0.125 to 0.125
- w_value: bfloat16 [2048, 1024], P(None, 'tp'), may hold values from -0.125 to 0.125
- w_delta_gate: bfloat16 [2048, 1024], P(None, 'tp'), may hold values from -0.125 to 0.125
- w_glu_value: bfloat16 [2048, 1024], P(None, 'tp'), may hold values from -0.125 to 0.125
- w_glu_gate: bfloat16 [2048, 1024], P(None, 'tp'), may hold values from -0.125 to 0.125
- w_conv_gate: bfloat16 [2048, 1024], P(None, 'tp'), may hold values from -0.125 to 0.125
- w_beta: bfloat16 [2048, 8], replicated, may hold values from -0.125 to 0.125
- w_decay: bfloat16 [2048, 8], replicated, may hold values from -0.125 to 0.125
- decay_log: float32 [8], replicated, may hold values from -12 to -3
- head_gain: float32 [128], replicated, may hold values from 0.1 to 1.9
- conv_taps: bfloat16 [31, 1024], P(None, 'tp'), may hold values from -2.5 to 2.5
- ln_gain: float32 [1024], P('tp'), may hold values from 0.1 to 1.9
- ln_shift: float32 [1024], P('tp'), may hold values from -3 to 3
- out_delta: bfloat16 [1024, 2048], P('tp'), may hold values from -0.125 to 0.125
- out_conv: bfloat16 [1024, 2048], P('tp'), may hold values from -0.125 to 0.125
Outputs:
- mixed_out: bfloat16 [32768, 2048], P(('sp', 'tp'))
All inputs are finite; a program needn't handle non-finite values.
Results may differ from a plain program's by a relative error of at most 0.024.
Values may be sent and summed in bfloat16 or wider, within the bound.
No kernel may reach another device: no remote copies, remote signals or barrier semaphores. Data moves between devices by JAX's collectives and lax.ppermute only.
A program may use at most 64 MiB of HBM per device.

v0:
```python
import jax
import jax.numpy as jnp
from jax import lax
from jax.sharding import Mesh
from jax.sharding import PartitionSpec as P

SPAN = 64
SP = ("sp_0", "sp_1")
SP_TP = ("sp_0", "sp_1", "tp")
TINY_NORM = 1e-06
TINY_VAR = 1e-05


def filled_with(shard, identity):
    return jnp.broadcast_to(jnp.asarray(identity, shard.dtype), shard.shape)


def prefix_by_axis(shard, axes, combine, identity):
    before = start = filled_with(shard, identity)
    so_far = shard
    for axis in reversed(axes):
        count, mine = (lax.axis_size(axis), lax.axis_index(axis))
        pieces = lax.all_gather(so_far, axis)
        inside, so_far = (start, start)
        for k in range(count):
            passed = k < mine
            so_far = combine(so_far, pieces[k])
            inside = jnp.where(passed, so_far, inside)
        before = combine(inside, before)
    return before


def shifted(block, axis, distance):
    devices = range(lax.axis_size(axis))
    route = [(i - distance, i) for i in devices if i - distance in devices]
    return lax.ppermute(block, axis, route)


def sent_to_all(shard, axis):
    count = lax.axis_size(axis)
    return lax.all_to_all(
        jnp.broadcast_to(shard[None], (count, *shard.shape)), axis, 0, 0, tiled=True
    )


def over_copies(shard, axis):
    return sent_to_all(shard, axis).sum(axis=0)


def packed_total(arrays, axis):
    ends = [0]
    for a in arrays:
        ends.append(ends[-1] + a.size)
    so_far = over_copies(jnp.concatenate([a.ravel() for a in arrays]), axis)
    return tuple((so_far[b:e].reshape(a.shape) for a, b, e in zip(arrays, ends, ends[1:])))


def block_terms(query, keys, values, strength, log_decay):
    log_sum = jnp.cumsum(log_decay, axis=-1)
    offsets = jnp.arange(SPAN)
    causal = offsets[:, None] >= offsets[None, :]
    strict = offsets[:, None] > offsets[None, :]
    spread = log_sum[..., :, None] - log_sum[..., None, :]
    damping = jnp.where(causal, jnp.exp(jnp.where(causal, spread, 0.0)), 0.0)
    scaled_keys = keys * strength[..., None]
    lower = jnp.where(strict, jnp.einsum("hnid,hnjd->hnij", scaled_keys, keys) * damping, 0.0)
    identity = jnp.eye(SPAN, dtype=jnp.float32)
    right = jnp.concatenate(
        [values * strength[..., None], scaled_keys * jnp.exp(log_sum)[..., None]], axis=-1
    )
    solved = jax.scipy.linalg.solve_triangular(
        identity + lower, right, lower=True, unit_diagonal=True
    )
    width = values.shape[-1]
    scores = jnp.einsum("hnid,hnjd->hnij", query, keys) * damping
    return (log_sum, solved[..., :width], solved[..., width:], scores)


def local(
    tokens,
    w_query,
    w_key,
    w_value,
    w_delta_gate,
    w_glu_value,
    w_glu_gate,
    w_conv_gate,
    w_beta,
    w_decay,
    decay_log,
    head_gain,
    conv_taps,
    ln_gain,
    ln_shift,
    out_delta,
    out_conv,
):
    rows_here = tokens.shape[0]
    tp_size = lax.axis_size("tp")
    width_all = tokens.shape[1] * tp_size
    weights = (
        w_query,
        w_key,
        w_value,
        w_delta_gate,
        w_glu_value,
        w_glu_gate,
        w_conv_gate,
        w_beta,
        w_decay,
    )
    piece = lax.all_gather(tokens, "tp", axis=1, tiled=True)
    totals = tuple(
        (jnp.dot(piece, weight, preferred_element_type=jnp.float32) for weight in weights)
    )
    squares = jnp.sum(jnp.square(piece.astype(jnp.float32)), axis=1)
    sums, squares = (totals, squares)
    inv_rms = lax.rsqrt(squares / width_all + TINY_NORM)[:, None]
    scaled = [summed * inv_rms for summed in sums]
    query_raw, key_raw, value_raw, delta_gate_raw, glu_value_raw, glu_gate_raw, conv_gate_raw = [
        item.astype(jnp.bfloat16) for item in scaled[:7]
    ]
    head_size = head_gain.shape[0]
    heads_here = w_query.shape[1] // head_size
    first_head = lax.axis_index("tp") * heads_here
    strength = jax.nn.sigmoid(lax.dynamic_slice_in_dim(scaled[7], first_head, heads_here, 1))
    rates = jnp.exp(lax.dynamic_slice_in_dim(decay_log, first_head, heads_here, 0))
    log_decay = -rates[None, :] * jax.nn.softplus(
        lax.dynamic_slice_in_dim(scaled[8], first_head, heads_here, 1)
    )
    blocks = rows_here // SPAN

    def to_blocks(raw):
        return jnp.transpose(raw.reshape(blocks, SPAN, heads_here, head_size), (2, 0, 1, 3))

    def unit_rows(array):
        return array * lax.rsqrt(jnp.sum(array * array, axis=-1, keepdims=True) + TINY_NORM)

    query = unit_rows(to_blocks(query_raw.astype(jnp.float32))) * head_size ** (-0.5)
    keys = unit_rows(to_blocks(key_raw.astype(jnp.float32)))
    values = to_blocks(value_raw.astype(jnp.float32))
    strength_blocks = jnp.transpose(strength.reshape(blocks, SPAN, heads_here), (2, 0, 1))
    decay_blocks = jnp.transpose(log_decay.reshape(blocks, SPAN, heads_here), (2, 0, 1))
    log_sum, corrected, key_terms, scores = block_terms(
        query, keys, values, strength_blocks, decay_blocks
    )

    def advance(memory, inputs):
        query_block, keys_block, corrected_block, terms_block, scores_block, log_block = inputs
        extended = jnp.concatenate([jnp.zeros_like(corrected_block), corrected_block], axis=-1)
        fresh = extended - jnp.einsum("hcd,hde->hce", terms_block, memory)
        output = jnp.einsum("hcd,hde->hce", query_block * jnp.exp(log_block)[..., None], memory)
        output = output + jnp.einsum("hcs,hse->hce", scores_block, fresh)
        tail_log = log_block[:, -1:]
        weighted = keys_block * jnp.exp(tail_log - log_block)[..., None]
        memory = memory * jnp.exp(tail_log)[..., None] + jnp.einsum("hcd,hce->hde", weighted, fresh)
        return (memory, output)

    start_state = jnp.concatenate(
        [
            jnp.broadcast_to(
                jnp.eye(head_size, dtype=jnp.float32), (heads_here, head_size, head_size)
            ),
            jnp.zeros((heads_here, head_size, head_size), jnp.float32),
        ],
        axis=-1,
    )
    sequence_inputs = tuple(
        (jnp.moveaxis(item, 1, 0) for item in (query, keys, corrected, key_terms, scores, log_sum))
    )
    final, outputs = lax.scan(advance, start_state, sequence_inputs)
    outputs = jnp.moveaxis(outputs, 0, 1).reshape(heads_here, rows_here, 2 * head_size)

    def compose(earlier, later):
        moved = jnp.einsum("hij,hjk->hik", later[..., :head_size], earlier)
        return moved + jnp.concatenate(
            [jnp.zeros_like(later[..., :head_size]), later[..., head_size:]], axis=-1
        )

    prefix = prefix_by_axis(final, SP, compose, start_state)
    carried = prefix[..., head_size:]
    result = outputs[..., head_size:] + jnp.einsum(
        "htd,hde->hte", outputs[..., :head_size], carried
    )
    result = jnp.transpose(result, (1, 0, 2))
    result = (
        result
        * lax.rsqrt(jnp.mean(result * result, axis=-1, keepdims=True) + TINY_NORM)
        * head_gain
    )
    delta_mixed = (
        result.reshape(rows_here, heads_here * head_size)
        * jax.nn.silu(delta_gate_raw.astype(jnp.float32))
    ).astype(jnp.bfloat16)
    kernel = conv_taps.shape[0]
    channels = conv_taps.shape[1]
    gated_units = (
        glu_value_raw.astype(jnp.float32) * jax.nn.sigmoid(glu_gate_raw.astype(jnp.float32))
    ).astype(jnp.bfloat16)
    before = shifted(gated_units[rows_here - (kernel - 1) :], SP, 1)
    padded = jnp.concatenate([before, gated_units], axis=0)
    filtered = jnp.zeros((rows_here, channels), jnp.float32)
    for offset in range(kernel):
        filtered = filtered + padded[offset : offset + rows_here].astype(jnp.float32) * conv_taps[
            offset
        ].astype(jnp.float32)
    first_sum = jnp.sum(filtered, axis=1)
    second_sum = jnp.sum(filtered * filtered, axis=1)
    first_sum, second_sum = packed_total((first_sum, second_sum), "tp")
    channels_all = channels * tp_size
    center = first_sum / channels_all
    variance = jnp.maximum(second_sum / channels_all - center * center, 0.0)
    normed = (filtered - center[:, None]) * lax.rsqrt(variance + TINY_VAR)[
        :, None
    ] * ln_gain + ln_shift
    conv_mixed = (jax.nn.silu(normed) * jax.nn.silu(conv_gate_raw.astype(jnp.float32))).astype(
        jnp.bfloat16
    )
    summed = jnp.dot(delta_mixed, out_delta, preferred_element_type=jnp.float32)
    return lax.psum_scatter(
        (summed + jnp.dot(conv_mixed, out_conv, preferred_element_type=jnp.float32)).astype(
            jnp.bfloat16
        ),
        "tp",
        scatter_dimension=0,
        tiled=True,
    )


def solution(mesh):
    finer = Mesh(mesh.devices.reshape(8, 4, mesh.shape["tp"]), ("sp_0", "sp_1", "tp"))
    placed = (
        P(SP, "tp"),
        P(None, "tp"),
        P(None, "tp"),
        P(None, "tp"),
        P(None, "tp"),
        P(None, "tp"),
        P(None, "tp"),
        P(None, "tp"),
        P(),
        P(),
        P(),
        P(),
        P(None, "tp"),
        P("tp"),
        P("tp"),
        P("tp", None),
        P("tp", None),
    )
    return jax.shard_map(
        local, mesh=finer, in_specs=placed, out_specs=P(SP_TP, None), check_vma=False
    )
```

profile of v0, /device:TPU:2, one launch (start us, length us, event | category | flops | bytes accessed | tf_op | source)
XLA Modules:
  0.0 365.5 jit_solution(16131292923218178079)
XLA Ops:
  7.3 1.2 dynamic_slice.30
  9.4 1.7 bitcast_convert_fusion.30
  11.1 39.1 %all-gather.5.cloned.1.call-done = bf16[1024,2048]{1,0:T(8,128)(2,1)} async-done(((bf16[1024,256]{1,0:T(8,128)(2,1)}), bf16[1024,2048]{1,0:T(8,128)(2,1)}) %all-gather.5.cloned.1.call-update) | async-done | bytes 4194320 | tf_op jit(solution)/shard_map/all_gather | solution.py:112
  50.2 3.2 multiply_reduce_fusion
  53.7 1.2 fusion.198
  54.9 1.2 fusion.197
  56.5 3.5 multiply_reduce_fusion.4
  60.8 78.6 %custom-call.4 = f32[16,1,64,64]{2,3,1,0:T(8,128)S(1)} custom-call(f32[16,1,64,64]{3,2,1,0:T(8,128)S(1)} %fusion.30), custom_call_target="InvertDiagBlocksLowerTriangular" | custom-call | tf_op jit(solution)/shard_map/jit(_solve_triangular)/vmap()/triangular_solve | solution.py:71
  139.5 3.6 fusion.34
  143.6 1.0 convolution_bitcast_fusion.2
  145.3 1.3 multiply_reduce_fusion.3
  146.8 1.2 fusion.25
  148.0 1.0 multiply_multiply_fusion
  149.1 84.6 %while.12 = (s32[]{:T(128)}, f32[1,128,256]{2,1,0:T(8,128)S(1)}, f32[16,1,64,256]{3,2,1,0:T(8,128)}, f32[16,1,64]{2,1,0:T(1,128)}, f32[16,1,64,128]{3,2,1,0:T(8,...) while((s32[]{:T(128)}, f32[1,128,256]{2,1,0:T(8,128)S(1)}, ...), condition=%wide.region_5.6_spmd, body=%wide.region_4.5_spmd.sunk | while | flops 14811202 | bytes 1019293 | solution.py:171
  151.0 1.2 exponential_bitcast_fusion.3
  152.9 1.5 fusion.250
  156.3 1.3 exponential_bitcast_fusion.3
  158.2 1.5 fusion.250
  161.6 1.3 exponential_bitcast_fusion.3
  163.5 1.5 fusion.250
  166.9 1.2 exponential_bitcast_fusion.3
  168.7 1.5 fusion.250
  172.2 1.3 exponential_bitcast_fusion.3
  174.1 1.5 fusion.250
  177.5 1.2 exponential_bitcast_fusion.3
  179.3 1.5 fusion.250
  182.7 1.2 exponential_bitcast_fusion.3
  184.5 1.5 fusion.250
  188.0 1.3 exponential_bitcast_fusion.3
  189.9 1.5 fusion.250
  193.3 1.3 exponential_bitcast_fusion.3
  195.2 1.5 fusion.250
  198.6 1.2 exponential_bitcast_fusion.3
  200.4 1.5 fusion.250
  203.8 1.2 exponential_bitcast_fusion.3
  205.6 1.5 fusion.250
  209.1 1.3 exponential_bitcast_fusion.3
  211.0 1.5 fusion.250
  214.3 1.2 exponential_bitcast_fusion.3
  216.1 1.5 fusion.250
  219.6 1.3 exponential_bitcast_fusion.3
  221.5 1.5 fusion.250
  224.9 1.3 exponential_bitcast_fusion.3
  226.9 1.5 fusion.250
  230.3 1.3 exponential_bitcast_fusion.3
  232.2 1.5 fusion.250
  233.7 13.6 %all-gather = f32[4,128,256]{2,1,0:T(8,128)S(1)} all-gather(f32[1,128,256]{2,1,0:T(8,128)S(1)} %get-tuple-element.54), channel_id=2, replica_groups=mesh['sp_0'=8,'sp_1'=4,'tp'=8] {'sp_1'}, dimensions={0}, use_global_device_ids=true | all-gather | bytes 655360 | tf_op jit(solution)/shard_map/all_gather | solution.py:23
  248.6 3.6 fusion.48
  252.4 1.2 fusion.42
  253.7 2.1 collective-permute-start
  255.9 3.6 collective-permute-done
  259.6 2.7 fusion.188
  263.0 3.9 %all-to-all-start = ((f32[8,1,2048]{2,1,0:T(1,128)}), f32[8,1,2048]{2,1,0:T(1,128)S(1)}, u32[]{:S(2)}, u32[]{:S(2)}) async-start(f32[8,1,2048]{2,1,0:T(1,128)} %broadcast_in_dim.36), calls=%async_computation | async-start | bytes 131072 | tf_op jit(solution)/shard_map/all_to_all | solution.py:41
  267.2 5.4 %all-to-all-done = f32[8,1,2048]{2,1,0:T(1,128)S(1)} async-done(((f32[8,1,2048]{2,1,0:T(1,128)}), f32[8,1,2048]{2,1,0:T(1,128)S(1)}, u32[]{:S(2)}, u32[]{:S(2)}) %all-to-all-start) | async-done | bytes 65568 | tf_op jit(solution)/shard_map/all_to_all | solution.py:41
  272.6 15.2 %all-gather.7.cloned.1.call-done = f32[8,128,256]{2,1,0:T(8,128)} async-done(((f32[1,128,256]{2,1,0:T(8,128)}), f32[8,128,256]{2,1,0:T(8,128)}) %all-gather.7.cloned.1.call-update) | async-done | bytes 1048592 | tf_op jit(solution)/shard_map/all_gather | solution.py:23
  287.8 1.1 fusion.191
  289.9 1.0 fusion.54
  291.8 1.0 fusion.56
  292.8 1.0 fusion.57
  295.8 1.8 convolution_bitcast_fusion.4
  297.6 1.2 multiply_reduce_fusion.2
  298.9 9.9 %fusion.81 = f32[1024,2048]{1,0:T(8,128)} fusion(bf16[128,2048]{1,0:T(8,128)(2,1)S(1)} %copy-done, f32[1,1024,128]{2,1,0:T(8,128)S(1)} %get-tuple-element.168, bf16[1024,2048]{1,0:T(8,128)(2,1)} %all-gather.5.cloned.1.call-done, bf16[2048,128]{1,0:T(8,128)(2,1)S(1)} %copy-done.8, f32[128]{0:T(128)S(1)} %copy-done.44, f32[1024]{0:T(1024)S(1)} %add_rsqrt_fusion, ...), kind=kOutput, calls=%fused_computation.153 | convolution fusion | flops 1075183616 | bytes 14164480 | tf_op jit(solution)/shard_map/dot_general | solution.py:219
  308.9 11.0 %add_convert_fusion = bf16[1024,2048]{1,0:T(8,128)(2,1)} fusion(f32[1024,2048]{1,0:T(8,128)} %fusion.81, bf16[128,2048]{1,0:T(8,128)(2,1)S(1)} %copy-done.6, bf16[1024,2048]{1,0:T(8,128)(2,1)} %all-gather.5.cloned.1.call-done, bf16[2048,128]{1,0:T(8,128)(2,1)S(1)} %copy-done.7, f32[1024,128]{1,0:T(8,128)S(1)} %get-tuple-element.113, f32[128]{0:T(128)S(1)} %copy-done.42, ...), kind=kOutput, calls=%fused_computation.32 | convolution fusion | flops 1080164352 | bytes 18363392 | tf_op jit(solution)/shard_map/dot_general | solution.py:221
  319.9 39.1 %reduce-scatter.2.cloned.1.call-done = bf16[128,2048]{1,0:T(8,128)(2,1)} async-done(((bf16[1024,2048]{1,0:T(8,128)(2,1)}), bf16[128,2048]{1,0:T(8,128)(2,1)}) %reduce-scatter.2.cloned.1.call-update) | async-done | bytes 524304 | tf_op jit(solution)/shard_map/reduce_scatter | solution.py:220
  (237 shorter events, 40.3 us)
Async XLA Ops:
  6.5 292.3 %copy-start = (bf16[128,2048]{1,0:T(8,128)(2,1)S(1)}, bf16[128,2048]{1,0:T(8,128)(2,1)}, u32[]{:S(2)}) copy-start(bf16[128,2048]{1,0:T(8,128)(2,1)} %param.34) | copy-start | bytes 1572868
  6.5 46.9 %copy-start.18 = (bf16[2048,8]{0,1:T(8,128)(2,1)S(1)}, bf16[2048,8]{0,1:T(8,128)(2,1)}, u32[]{:S(2)}) copy-start(bf16[2048,8]{0,1:T(8,128)(2,1)} %param.27) | copy-start | bytes 98308
  6.5 43.7 %all-gather.5.cloned.1.call-start = ((), (), s32[]{:S(2)}) async-start(), calls=%async_computation.2 | async-start | bytes 4718592 | tf_op jit(solution)/shard_map/all_gather | solution.py:112
  7.3 280.5 %all-gather.7.cloned.1.call-start = ((), (), s32[]{:S(2)}) async-start(), calls=%async_computation.4 | async-start | bytes 1179648 | tf_op jit(solution)/shard_map/all_gather | solution.py:23
  9.3 50.8 %copy-start.21 = (pred[64,64]{1,0:T(8,128)(4,1)}, pred[64,64]{1,0:T(8,128)(4,1)S(1)}, u32[]{:S(2)}) copy-start(pred[64,64]{1,0:T(8,128)(4,1)S(1)} %get-tuple-element.169) | copy-start | bytes 12292
  50.2 3.4 copy-start.1
  50.2 4.6 %copy-start.19 = (bf16[2048,8]{0,1:T(8,128)(2,1)S(1)}, bf16[2048,8]{0,1:T(8,128)(2,1)}, u32[]{:S(2)}) copy-start(bf16[2048,8]{0,1:T(8,128)(2,1)} %param.28) | copy-start | bytes 98308
  53.7 85.8 %copy-start.10 = (f32[1024]{0:T(1024)}, f32[1024]{0:T(1024)S(1)}, u32[]{:S(2)}) copy-start(f32[1024]{0:T(1024)S(1)} %add_rsqrt_fusion.3) | copy-start | bytes 12292
  53.7 2.8 copy-start.45
  56.5 3.6 copy-start.15
  60.1 83.0 %copy-start.13 = (f32[16,64]{1,0:T(8,128)}, f32[16,64]{1,0:T(8,128)S(1)}, u32[]{:S(2)}) copy-start(f32[16,64]{1,0:T(8,128)S(1)} %rsqrt.42) | copy-start | bytes 12292
  143.0 2.2 copy-start.2
  143.0 2.2 copy-start.11
  143.0 2.3 copy-start.46
  144.6 2.1 copy-start.14
  144.6 2.1 copy-start.16
  144.6 2.1 copy-start.22
  146.8 1.2 copy-start.17
  149.0 99.5 %copy-start.12 = (f32[1024]{0:T(1024)S(1)}, f32[1024]{0:T(1024)}, u32[]{:S(2)}) copy-start(f32[1024]{0:T(1024)} %copy-done.10) | copy-start | bytes 12292
  149.0 99.5 %copy-start.47 = (bf16[2048,128]{1,0:T(8,128)(2,1)S(1)}, bf16[2048,128]{1,0:T(8,128)(2,1)}, u32[]{:S(2)}) copy-start(bf16[2048,128]{1,0:T(8,128)(2,1)} %param.25) | copy-start | bytes 1572868
  248.6 3.6 copy-start.3
  248.6 3.6 copy-start.5
  252.2 3.6 copy-start.20
  252.2 7.2 %copy-start.23 = (f32[128]{0:T(128)S(1)}, f32[128]{0:T(128)}, u32[]{:S(2)}) copy-start(f32[128]{0:T(128)} %get-tuple-element.130) | copy-start | bytes 1540
  252.2 7.2 %copy-start.24 = (f32[128]{0:T(128)S(1)}, f32[128]{0:T(128)}, u32[]{:S(2)}) copy-start(f32[128]{0:T(128)} %get-tuple-element.131) | copy-start | bytes 1540
  252.3 7.2 %copy-start.25 = (f32[128]{0:T(128)S(1)}, f32[128]{0:T(128)}, u32[]{:S(2)}) copy-start(f32[128]{0:T(128)} %get-tuple-element.132) | copy-start | bytes 1540
  252.3 7.2 %copy-start.26 = (f32[128]{0:T(128)S(1)}, f32[128]{0:T(128)}, u32[]{:S(2)}) copy-start(f32[128]{0:T(128)} %get-tuple-element.133) | copy-start | bytes 1540
  252.3 7.2 %copy-start.27 = (f32[128]{0:T(128)S(1)}, f32[128]{0:T(128)}, u32[]{:S(2)}) copy-start(f32[128]{0:T(128)} %get-tuple-element.134) | copy-start | bytes 1540
  252.3 7.2 %copy-start.28 = (f32[128]{0:T(128)S(1)}, f32[128]{0:T(128)}, u32[]{:S(2)}) copy-start(f32[128]{0:T(128)} %get-tuple-element.135) | copy-start | bytes 1540
  252.3 7.2 %copy-start.29 = (f32[128]{0:T(128)S(1)}, f32[128]{0:T(128)}, u32[]{:S(2)}) copy-start(f32[128]{0:T(128)} %get-tuple-element.136) | copy-start | bytes 1540
  252.3 7.2 %copy-start.30 = (f32[128]{0:T(128)S(1)}, f32[128]{0:T(128)}, u32[]{:S(2)}) copy-start(f32[128]{0:T(128)} %get-tuple-element.137) | copy-start | bytes 1540
  252.3 7.2 %copy-start.31 = (f32[128]{0:T(128)S(1)}, f32[128]{0:T(128)}, u32[]{:S(2)}) copy-start(f32[128]{0:T(128)} %get-tuple-element.138) | copy-start | bytes 1540
  252.3 7.2 %copy-start.32 = (f32[128]{0:T(128)S(1)}, f32[128]{0:T(128)}, u32[]{:S(2)}) copy-start(f32[128]{0:T(128)} %get-tuple-element.139) | copy-start | bytes 1540
  252.3 7.2 %copy-start.33 = (f32[128]{0:T(128)S(1)}, f32[128]{0:T(128)}, u32[]{:S(2)}) copy-start(f32[128]{0:T(128)} %get-tuple-element.140) | copy-start | bytes 1540
  252.3 7.2 %copy-start.34 = (f32[128]{0:T(128)S(1)}, f32[128]{0:T(128)}, u32[]{:S(2)}) copy-start(f32[128]{0:T(128)} %get-tuple-element.141) | copy-start | bytes 1540
  252.4 7.2 %copy-start.35 = (f32[128]{0:T(128)S(1)}, f32[128]{0:T(128)}, u32[]{:S(2)}) copy-start(f32[128]{0:T(128)} %get-tuple-element.142) | copy-start | bytes 1540
  252.4 7.2 %copy-start.36 = (f32[128]{0:T(128)S(1)}, f32[128]{0:T(128)}, u32[]{:S(2)}) copy-start(f32[128]{0:T(128)} %get-tuple-element.143) | copy-start | bytes 1540
  252.4 7.2 %copy-start.37 = (f32[128]{0:T(128)S(1)}, f32[128]{0:T(128)}, u32[]{:S(2)}) copy-start(f32[128]{0:T(128)} %get-tuple-element.144) | copy-start | bytes 1540
  252.4 7.2 %copy-start.38 = (f32[128]{0:T(128)S(1)}, f32[128]{0:T(128)}, u32[]{:S(2)}) copy-start(f32[128]{0:T(128)} %get-tuple-element.145) | copy-start | bytes 1540
  252.4 7.2 %copy-start.39 = (f32[128]{0:T(128)S(1)}, f32[128]{0:T(128)}, u32[]{:S(2)}) copy-start(f32[128]{0:T(128)} %get-tuple-element.146) | copy-start | bytes 1540
  252.4 7.2 %copy-start.40 = (f32[128]{0:T(128)S(1)}, f32[128]{0:T(128)}, u32[]{:S(2)}) copy-start(f32[128]{0:T(128)} %get-tuple-element.147) | copy-start | bytes 1540
  252.4 7.2 %copy-start.41 = (f32[128]{0:T(128)S(1)}, f32[128]{0:T(128)}, u32[]{:S(2)}) copy-start(f32[128]{0:T(128)} %get-tuple-element.148) | copy-start | bytes 1540
  252.4 14.5 %copy-start.4 = (f32[1,128,256]{2,1,0:T(8,128)S(1)}, f32[1,128,256]{2,1,0:T(8,128)}, u32[]{:S(2)}) copy-start(f32[1,128,256]{2,1,0:T(8,128)} %fusion.53) | copy-start | bytes 393220
  253.7 43.9 %copy-start.9 = (f32[16,1,64,256]{3,2,1,0:T(8,128)S(1)}, f32[16,1,64,256]{3,2,1,0:T(8,128)}, u32[]{:S(2)}) copy-start(f32[16,1,64,256]{3,2,1,0:T(8,128)} %get-tuple-element.53) | copy-start | bytes 3145732
  253.7 45.2 %copy-start.8 = (bf16[2048,128]{1,0:T(8,128)(2,1)S(1)}, bf16[2048,128]{1,0:T(8,128)(2,1)}, u32[]{:S(2)}) copy-start(bf16[2048,128]{1,0:T(8,128)(2,1)} %param.23) | copy-start | bytes 1572868
  253.7 45.2 %copy-start.44 = (f32[128]{0:T(128)S(1)}, f32[128]{0:T(128)}, u32[]{:S(2)}) copy-start(f32[128]{0:T(128)} %param.30) | copy-start | bytes 1540
  253.7 5.7 %collective-permute-start = (bf16[30,128]{1,0:T(8,128)(2,1)S(1)}, bf16[30,128]{1,0:T(8,128)(2,1)S(1)}, u32[]{:S(2)}, u32[]{:S(2)}) collective-permute-start(bf16[30,128]{1,0:T(8,128)(2,1)S(1)} %slice.504), channel_id=1, source_target_pairs={{0,8},{8,16},{16,24},{24,32},{32,40},{40,48},{48,56},{56,64},{64,7... | collective-permute-start | bytes 23048 | tf_op jit(solution)/shard_map/ppermute | solution.py:36
  263.0 9.6 %all-to-all-start = ((f32[8,1,2048]{2,1,0:T(1,128)}), f32[8,1,2048]{2,1,0:T(1,128)S(1)}, u32[]{:S(2)}, u32[]{:S(2)}) async-start(f32[8,1,2048]{2,1,0:T(1,128)} %broadcast_in_dim.36), calls=%async_computation | async-start | bytes 131072 | tf_op jit(solution)/shard_map/all_to_all | solution.py:41
  266.9 92.1 %reduce-scatter.2.cloned.1.call-start = ((), (), s32[]{:S(2)}) async-start(), calls=%async_computation.3 | async-start | bytes 4718592 | tf_op jit(solution)/shard_map/reduce_scatter | solution.py:220
  298.9 10.0 %copy-start.6 = (bf16[128,2048]{1,0:T(8,128)(2,1)S(1)}, bf16[128,2048]{1,0:T(8,128)(2,1)}, u32[]{:S(2)}) copy-start(bf16[128,2048]{1,0:T(8,128)(2,1)} %param.35) | copy-start | bytes 1572868
  298.9 10.0 %copy-start.7 = (bf16[2048,128]{1,0:T(8,128)(2,1)S(1)}, bf16[2048,128]{1,0:T(8,128)(2,1)}, u32[]{:S(2)}) copy-start(bf16[2048,128]{1,0:T(8,128)(2,1)} %param.26) | copy-start | bytes 1572868
  298.9 9.9 %copy-start.42 = (f32[128]{0:T(128)S(1)}, f32[128]{0:T(128)}, u32[]{:S(2)}) copy-start(f32[128]{0:T(128)} %param.33) | copy-start | bytes 1540
  298.9 9.9 %copy-start.43 = (f32[128]{0:T(128)S(1)}, f32[128]{0:T(128)}, u32[]{:S(2)}) copy-start(f32[128]{0:T(128)} %param.32) | copy-start | bytes 1540
Sparse Core Ops, SparseCore 0:
  9.2 41.0 all-gather.4
  248.7 39.0 all-gather.6
  320.0 38.9 reduce-scatter.1
where the time goes:
time: 368 us; the launch traced here: 366 us
  other arithmetic  108 us (29%)
  waiting for transfers between devices  103 us (28%)
  matrix products  84.4 us (23%)
  local copies, waits for them, and re-layouts  24.7 us (7%)
  between operations  14.6 us (4%)
  blocking collectives  13.6 us (4%)
  loops' own time  10.6 us (3%)
  starting transfers between devices  6.06 us (2%)
    another operation x4, other arithmetic, block_terms(): jax.scipy.linalg.solve_triangular(identity + lower, right, lower=True, un...  78.7 us
    reduce_scatter x1, waiting for transfers between devices, local(): lax.psum_scatter((summed + jnp.dot(conv_mixed, out_conv, preferred_elemen...  39.1 us
    all_gather x1, waiting for transfers between devices, local(): piece = lax.all_gather(tokens, 'tp', axis=1, tiled=True)  39.1 us
    dot_general x16, matrix products, advance(): output = output + jnp.einsum('hcs,hse->hce', scores_block, fresh)  23.6 us
    exp x16, other arithmetic, advance(): jnp.exp(log_block)[..., None]  20.1 us
    dot_general x7, matrix products, local(): jnp.dot(piece, weight, preferred_element_type=jnp.float32)  15.6 us
    all_gather x1, waiting for transfers between devices, prefix_by_axis(): pieces = lax.all_gather(so_far, axis)  15.2 us
    all_gather x1, blocking collectives, prefix_by_axis(): pieces = lax.all_gather(so_far, axis)  13.6 us
  transfers between devices with their start and end apart: 5, of which 5 were waited for; matrix products, arithmetic and copies ran while one was open for 3% of the time, Pallas kernels for 0%

commit v1 on v0

--- a/solution.py
+++ b/solution.py
@@ -9,6 +9,13 @@
 SP_TP = ("sp_0", "sp_1", "tp")
 TINY_NORM = 1e-06
 TINY_VAR = 1e-05
+
+
+def exchange_gather(x, mesh_axis, dim):
+    devices = lax.axis_size(mesh_axis)
+    tiles = jnp.stack([x for _ in range(devices)])
+    tiles = lax.all_to_all(tiles, mesh_axis, split_axis=0, concat_axis=0)
+    return jnp.concatenate(tiles, axis=dim)
 
 
 def filled_with(shard, identity):
@@ -109,7 +116,7 @@
         w_beta,
         w_decay,
     )
-    piece = lax.all_gather(tokens, "tp", axis=1, tiled=True)
+    piece = exchange_gather(tokens, "tp", 1)
     totals = tuple(
         (jnp.dot(piece, weight, preferred_element_type=jnp.float32) for weight in weights)
     )

time: 368 us -> 391 us (1.062)
  matrix products: 84.4 us -> 92.8 us
  starting transfers between devices: 6.06 us -> 12.4 us
  waiting for transfers between devices: 103 us -> 107 us
    all_to_all x0 -> x1, waiting for transfers between devices: none -> 47.4 us  [exchange_gather(): tiles = lax.all_to_all(tiles, mesh_axis, split_axis=0, concat_axis=0)]
    all_gather x1 -> x0, waiting for transfers between devices: 39.1 us -> none  [local(): piece = lax.all_gather(tokens, 'tp', axis=1, tiled=True)]
    dot_general x7, matrix products: 15.6 us -> 23.8 us  [local(): jnp.dot(piece, weight, preferred_element_type=jnp.float32)]
    all_to_all x0 -> x1, starting transfers between devices: none -> 4.72 us  [exchange_gather(): tiles = lax.all_to_all(tiles, mesh_axis, split_axis=0, concat_axis=0)]
where the time goes in v1:
time: 391 us; the launch traced here: 388 us
  other arithmetic  108 us (28%)
  waiting for transfers between devices  107 us (27%)
  matrix products  92.8 us (24%)
  local copies, waits for them, and re-layouts  27.5 us (7%)
  between operations  14.9 us (4%)
  blocking collectives  13 us (3%)
  starting transfers between devices  12.4 us (3%)
  loops' own time  11.9 us (3%)
    another operation x4, other arithmetic, block_terms(): jax.scipy.linalg.solve_triangular(identity + lower, right, lower=True, un...  78.7 us
    all_to_all x1, waiting for transfers between devices, exchange_gather(): tiles = lax.all_to_all(tiles, mesh_axis, split_axis=0, concat_axis=0)  47.4 us
    reduce_scatter x1, waiting for transfers between devices, local(): lax.psum_scatter((summed + jnp.dot(conv_mixed, out_conv, preferred_elemen...  39.1 us
    dot_general x7, matrix products, local(): jnp.dot(piece, weight, preferred_element_type=jnp.float32)  23.8 us
    dot_general x16, matrix products, advance(): output = output + jnp.einsum('hcs,hse->hce', scores_block, fresh)  23.7 us
    exp x16, other arithmetic, advance(): jnp.exp(log_block)[..., None]  21.2 us
    all_gather x1, waiting for transfers between devices, prefix_by_axis(): pieces = lax.all_gather(so_far, axis)  13.9 us
    all_gather x1, blocking collectives, prefix_by_axis(): pieces = lax.all_gather(so_far, axis)  13 us
  transfers between devices with their start and end apart: 5, of which 5 were waited for; matrix products, arithmetic and copies ran while one was open for 3% of the time, Pallas kernels for 0%

profile of v1, /device:TPU:2, one launch (start us, length us, event | category | flops | bytes accessed | tf_op | source)
XLA Modules:
  0.0 388.2 jit_solution(10961715103665539064)
XLA Ops:
  6.5 1.3 copy.53
  7.8 2.5 stack.2
  10.4 4.7 %all-to-all-start = ((bf16[8,1024,256]{1,2,0:T(8,128)(2,1)}), bf16[8,1024,256]{1,2,0:T(8,128)(2,1)}, u32[]{:S(2)}, u32[]{:S(2)}) async-start(bf16[8,1024,256]{1,2,0:T(8,128)(2,1)} %stack.2), calls=%async_computation | async-start | bytes 8388608 | tf_op jit(solution)/shard_map/all_to_all | solution.py:17
  17.3 47.4 %all-to-all-done = bf16[8,1024,256]{1,2,0:T(8,128)(2,1)} async-done(((bf16[8,1024,256]{1,2,0:T(8,128)(2,1)}), bf16[8,1024,256]{1,2,0:T(8,128)(2,1)}, u32[]{:S(2)}, u32[]{:S(2)}) %all-to-all-start) | async-done | bytes 4194336 | tf_op jit(solution)/shard_map/all_to_all | solution.py:17
  64.7 3.1 multiply_reduce_fusion
  67.9 2.9 fusion.198
  70.8 2.9 fusion.197
  74.1 3.5 fusion.34
  77.6 3.6 multiply_reduce_fusion.4
  82.0 78.6 %custom-call.4 = f32[16,1,64,64]{2,3,1,0:T(8,128)S(1)} custom-call(f32[16,1,64,64]{3,2,1,0:T(8,128)S(1)} %fusion.30), custom_call_target="InvertDiagBlocksLowerTriangular" | custom-call | tf_op jit(solution)/shard_map/jit(_solve_triangular)/vmap()/triangular_solve | solution.py:78
  161.2 1.1 convolution_bitcast_fusion.2
  162.3 3.8 multiply_reduce_fusion.3
  166.2 1.2 fusion.25
  167.4 1.0 multiply_multiply_fusion
  168.5 87.7 %while.12 = (s32[]{:T(128)}, f32[1,128,256]{2,1,0:T(8,128)S(1)}, f32[16,1,64,256]{3,2,1,0:T(8,128)}, f32[16,1,64]{2,1,0:T(1,128)}, f32[16,1,64,128]{3,2,1,0:T(8,...) while((s32[]{:T(128)}, f32[1,128,256]{2,1,0:T(8,128)S(1)}, ...), condition=%wide.region_5.6_spmd, body=%wide.region_4.5_spmd.sunk | while | flops 14811202 | bytes 1019293 | solution.py:178
  170.6 1.3 exponential_bitcast_fusion.3
  172.5 1.5 fusion.250
  176.0 1.3 exponential_bitcast_fusion.3
  178.0 1.5 fusion.250
  181.5 1.4 exponential_bitcast_fusion.3
  183.6 1.5 fusion.250
  187.0 1.3 exponential_bitcast_fusion.3
  189.0 1.5 fusion.250
  192.5 1.3 exponential_bitcast_fusion.3
  194.4 1.5 fusion.250
  197.8 1.3 exponential_bitcast_fusion.3
  199.7 1.5 fusion.250
  203.2 1.3 exponential_bitcast_fusion.3
  205.2 1.5 fusion.250
  208.7 1.4 exponential_bitcast_fusion.3
  210.7 1.5 fusion.250
  214.2 1.4 exponential_bitcast_fusion.3
  216.2 1.5 fusion.250
  219.7 1.3 exponential_bitcast_fusion.3
  221.7 1.5 fusion.250
  225.2 1.3 exponential_bitcast_fusion.3
  227.1 1.5 fusion.250
  230.7 1.4 exponential_bitcast_fusion.3
  232.7 1.5 fusion.250
  236.2 1.3 exponential_bitcast_fusion.3
  238.1 1.5 fusion.250
  241.7 1.4 exponential_bitcast_fusion.3
  243.7 1.5 fusion.250
  247.3 1.4 exponential_bitcast_fusion.3
  249.3 1.5 fusion.250
  252.7 1.3 exponential_bitcast_fusion.3
  254.7 1.5 fusion.250
  256.1 13.0 %all-gather = f32[4,128,256]{2,1,0:T(8,128)S(1)} all-gather(f32[1,128,256]{2,1,0:T(8,128)S(1)} %get-tuple-element.54), channel_id=2, replica_groups=mesh['sp_0'=8,'sp_1'=4,'tp'=8] {'sp_1'}, dimensions={0}, use_global_device_ids=true | all-gather | bytes 655360 | tf_op jit(solution)/shard_map/all_gather | solution.py:30
  270.5 3.6 fusion.48
  274.3 3.5 fusion.42
  277.9 4.3 %collective-permute-start = (bf16[30,128]{1,0:T(8,128)(2,1)S(1)}, bf16[30,128]{1,0:T(8,128)(2,1)S(1)}, u32[]{:S(2)}, u32[]{:S(2)}) collective-permute-start(bf16[30,128]{1,0:T(8,128)(2,1)S(1)} %slice.504), channel_id=1, source_target_pairs={{0,8},{8,16},{16,24},{24,32},{32,40},{40,48},{48,56},{56,64},{64,7... | collective-permute-start | bytes 23048 | tf_op jit(solution)/shard_map/ppermute | solution.py:43
  282.2 1.5 collective-permute-done
  283.9 2.7 fusion.188
  287.3 3.3 all-to-all-start.1
  290.9 5.3 %all-to-all-done.1 = f32[8,1,2048]{2,1,0:T(1,128)S(1)} async-done(((f32[8,1,2048]{2,1,0:T(1,128)}), f32[8,1,2048]{2,1,0:T(1,128)S(1)}, u32[]{:S(2)}, u32[]{:S(2)}) %all-to-all-start.1) | async-done | bytes 65568 | tf_op jit(solution)/shard_map/all_to_all | solution.py:48
  296.3 13.9 %all-gather.4.cloned.1.call-done = f32[8,128,256]{2,1,0:T(8,128)} async-done(((f32[1,128,256]{2,1,0:T(8,128)}), f32[8,128,256]{2,1,0:T(8,128)}) %all-gather.4.cloned.1.call-update) | async-done | bytes 1048592 | tf_op jit(solution)/shard_map/all_gather | solution.py:30
  310.2 1.1 fusion.191
  312.3 1.0 fusion.54
  314.3 1.0 fusion.56
  318.2 1.8 convolution_bitcast_fusion.4
  320.1 1.2 multiply_reduce_fusion.2
  321.4 9.9 %fusion.81 = f32[1024,2048]{1,0:T(8,128)} fusion(bf16[128,2048]{1,0:T(8,128)(2,1)S(1)} %copy-done, f32[1,1024,128]{2,1,0:T(8,128)S(1)} %get-tuple-element.177, bf16[1024,2048]{0,1:T(8,128)(2,1)} %bitcast.17, bf16[2048,128]{1,0:T(8,128)(2,1)S(1)} %copy-done.5, f32[128]{0:T(128)S(1)} %copy-done.37, f32[1024]{0:T(1024)S(1)} %add_rsqrt_fusion, ...), kind=kOutput, calls=%fused_computation.153 | convolution fusion | flops 1075183616 | bytes 14164480 | tf_op jit(solution)/shard_map/dot_general | solution.py:226
  331.3 11.0 %add_convert_fusion = bf16[1024,2048]{1,0:T(8,128)(2,1)} fusion(f32[1024,2048]{1,0:T(8,128)} %fusion.81, bf16[128,2048]{1,0:T(8,128)(2,1)S(1)} %copy-done.3, bf16[1024,2048]{0,1:T(8,128)(2,1)} %bitcast.17, bf16[2048,128]{1,0:T(8,128)(2,1)S(1)} %copy-done.4, f32[1024,128]{1,0:T(8,128)S(1)} %get-tuple-element.122, f32[128]{0:T(128)S(1)} %copy-done.35, ...), kind=kOutput, calls=%fused_computation.32 | convolution fusion | flops 1080164352 | bytes 18363392 | tf_op jit(solution)/shard_map/dot_general | solution.py:228
  342.3 39.1 %reduce-scatter.2.cloned.1.call-done = bf16[128,2048]{1,0:T(8,128)(2,1)} async-done(((bf16[1024,2048]{1,0:T(8,128)(2,1)}), bf16[128,2048]{1,0:T(8,128)(2,1)}) %reduce-scatter.2.cloned.1.call-update) | async-done | bytes 524304 | tf_op jit(solution)/shard_map/reduce_scatter | solution.py:227
  (226 shorter events, 41.5 us)
Async XLA Ops:
  6.5 314.8 %copy-start = (bf16[128,2048]{1,0:T(8,128)(2,1)S(1)}, bf16[128,2048]{1,0:T(8,128)(2,1)}, u32[]{:S(2)}) copy-start(bf16[128,2048]{1,0:T(8,128)(2,1)} %param.34) | copy-start | bytes 1572868
  10.3 4.8 %copy-start.41 = (f32[8]{0:T(128)S(1)}, f32[8]{0:T(128)}, u32[]{:S(2)}) copy-start(f32[8]{0:T(128)} %param.29) | copy-start | bytes 100
  10.3 6.2 %copy-start.14 = (bf16[31,128]{1,0:T(8,128)(2,1)S(1)}, bf16[31,128]{1,0:T(8,128)(2,1)}, u32[]{:S(2)}) copy-start(bf16[31,128]{1,0:T(8,128)(2,1)} %param.31) | copy-start | bytes 23812
  10.4 54.4 %all-to-all-start = ((bf16[8,1024,256]{1,2,0:T(8,128)(2,1)}), bf16[8,1024,256]{1,2,0:T(8,128)(2,1)}, u32[]{:S(2)}, u32[]{:S(2)}) async-start(bf16[8,1024,256]{1,2,0:T(8,128)(2,1)} %stack.2), calls=%async_computation | async-start | bytes 8388608 | tf_op jit(solution)/shard_map/all_to_all | solution.py:17
  15.1 52.8 %copy-start.11 = (bf16[2048,8]{0,1:T(8,128)(2,1)S(1)}, bf16[2048,8]{0,1:T(8,128)(2,1)}, u32[]{:S(2)}) copy-start(bf16[2048,8]{0,1:T(8,128)(2,1)} %param.27) | copy-start | bytes 98308
  15.1 295.1 %all-gather.4.cloned.1.call-start = ((), (), s32[]{:S(2)}) async-start(), calls=%async_computation.4 | async-start | bytes 1179648 | tf_op jit(solution)/shard_map/all_gather | solution.py:30
  17.3 53.5 %copy-start.12 = (bf16[2048,8]{0,1:T(8,128)(2,1)S(1)}, bf16[2048,8]{0,1:T(8,128)(2,1)}, u32[]{:S(2)}) copy-start(bf16[2048,8]{0,1:T(8,128)(2,1)} %param.28) | copy-start | bytes 98308
  67.8 94.5 %copy-start.6 = (f32[1024]{0:T(1024)}, f32[1024]{0:T(1024)S(1)}, u32[]{:S(2)}) copy-start(f32[1024]{0:T(1024)S(1)} %add_rsqrt_fusion.3) | copy-start | bytes 12292
  67.9 6.2 %copy-start.38 = (bf16[2048,128]{1,0:T(8,128)(2,1)S(1)}, bf16[2048,128]{1,0:T(8,128)(2,1)}, u32[]{:S(2)}) copy-start(bf16[2048,128]{1,0:T(8,128)(2,1)} %param.22) | copy-start | bytes 1572868
  70.8 6.8 %copy-start.39 = (bf16[2048,128]{1,0:T(8,128)(2,1)S(1)}, bf16[2048,128]{1,0:T(8,128)(2,1)}, u32[]{:S(2)}) copy-start(bf16[2048,128]{1,0:T(8,128)(2,1)} %param.21) | copy-start | bytes 1572868
  74.1 92.1 %copy-start.10 = (f32[1,16,64]{2,1,0:T(8,128)}, f32[1,16,64]{2,1,0:T(8,128)S(1)}, u32[]{:S(2)}) copy-start(f32[1,16,64]{2,1,0:T(8,128)S(1)} %reduce_window_sum.11) | copy-start | bytes 12292
  81.3 84.9 %copy-start.9 = (f32[16,64]{1,0:T(8,128)}, f32[16,64]{1,0:T(8,128)S(1)}, u32[]{:S(2)}) copy-start(f32[16,64]{1,0:T(8,128)S(1)} %rsqrt.42) | copy-start | bytes 12292
  166.2 1.2 copy-start.13
  168.5 102.0 %copy-start.7 = (f32[1024]{0:T(1024)S(1)}, f32[1024]{0:T(1024)}, u32[]{:S(2)}) copy-start(f32[1024]{0:T(1024)} %copy-done.6) | copy-start | bytes 12292
  168.5 102.0 %copy-start.40 = (bf16[2048,128]{1,0:T(8,128)(2,1)S(1)}, bf16[2048,128]{1,0:T(8,128)(2,1)}, u32[]{:S(2)}) copy-start(bf16[2048,128]{1,0:T(8,128)(2,1)} %param.25) | copy-start | bytes 1572868
  270.5 3.6 copy-start.2
  274.1 8.1 %copy-start.15 = (bf16[31,128]{1,0:T(8,128)(2,1)S(1)}, bf16[31,128]{1,0:T(8,128)(2,1)}, u32[]{:S(2)}) copy-start(bf16[31,128]{1,0:T(8,128)(2,1)} %param.31) | copy-start | bytes 23812
  274.1 9.6 %copy-start.16 = (f32[128]{0:T(128)S(1)}, f32[128]{0:T(128)}, u32[]{:S(2)}) copy-start(f32[128]{0:T(128)} %get-tuple-element.139) | copy-start | bytes 1540
  274.1 9.6 %copy-start.17 = (f32[128]{0:T(128)S(1)}, f32[128]{0:T(128)}, u32[]{:S(2)}) copy-start(f32[128]{0:T(128)} %get-tuple-element.140) | copy-start | bytes 1540
  274.1 9.6 %copy-start.18 = (f32[128]{0:T(128)S(1)}, f32[128]{0:T(128)}, u32[]{:S(2)}) copy-start(f32[128]{0:T(128)} %get-tuple-element.141) | copy-start | bytes 1540
  274.1 9.6 %copy-start.19 = (f32[128]{0:T(128)S(1)}, f32[128]{0:T(128)}, u32[]{:S(2)}) copy-start(f32[128]{0:T(128)} %get-tuple-element.142) | copy-start | bytes 1540
  274.2 9.6 %copy-start.20 = (f32[128]{0:T(128)S(1)}, f32[128]{0:T(128)}, u32[]{:S(2)}) copy-start(f32[128]{0:T(128)} %get-tuple-element.143) | copy-start | bytes 1540
  274.2 9.6 %copy-start.21 = (f32[128]{0:T(128)S(1)}, f32[128]{0:T(128)}, u32[]{:S(2)}) copy-start(f32[128]{0:T(128)} %get-tuple-element.144) | copy-start | bytes 1540
  274.2 9.6 %copy-start.22 = (f32[128]{0:T(128)S(1)}, f32[128]{0:T(128)}, u32[]{:S(2)}) copy-start(f32[128]{0:T(128)} %get-tuple-element.145) | copy-start | bytes 1540
  274.2 9.6 %copy-start.23 = (f32[128]{0:T(128)S(1)}, f32[128]{0:T(128)}, u32[]{:S(2)}) copy-start(f32[128]{0:T(128)} %get-tuple-element.146) | copy-start | bytes 1540
  274.2 9.6 %copy-start.24 = (f32[128]{0:T(128)S(1)}, f32[128]{0:T(128)}, u32[]{:S(2)}) copy-start(f32[128]{0:T(128)} %get-tuple-element.147) | copy-start | bytes 1540
  274.2 9.6 %copy-start.25 = (f32[128]{0:T(128)S(1)}, f32[128]{0:T(128)}, u32[]{:S(2)}) copy-start(f32[128]{0:T(128)} %get-tuple-element.148) | copy-start | bytes 1540
  274.2 9.6 %copy-start.26 = (f32[128]{0:T(128)S(1)}, f32[128]{0:T(128)}, u32[]{:S(2)}) copy-start(f32[128]{0:T(128)} %get-tuple-element.149) | copy-start | bytes 1540
  274.2 9.6 %copy-start.27 = (f32[128]{0:T(128)S(1)}, f32[128]{0:T(128)}, u32[]{:S(2)}) copy-start(f32[128]{0:T(128)} %get-tuple-element.150) | copy-start | bytes 1540
  274.2 9.6 %copy-start.28 = (f32[128]{0:T(128)S(1)}, f32[128]{0:T(128)}, u32[]{:S(2)}) copy-start(f32[128]{0:T(128)} %get-tuple-element.151) | copy-start | bytes 1540
  274.2 9.6 %copy-start.29 = (f32[128]{0:T(128)S(1)}, f32[128]{0:T(128)}, u32[]{:S(2)}) copy-start(f32[128]{0:T(128)} %get-tuple-element.152) | copy-start | bytes 1540
  274.3 9.6 %copy-start.30 = (f32[128]{0:T(128)S(1)}, f32[128]{0:T(128)}, u32[]{:S(2)}) copy-start(f32[128]{0:T(128)} %get-tuple-element.153) | copy-start | bytes 1540
  274.3 9.6 %copy-start.31 = (f32[128]{0:T(128)S(1)}, f32[128]{0:T(128)}, u32[]{:S(2)}) copy-start(f32[128]{0:T(128)} %get-tuple-element.154) | copy-start | bytes 1540
  274.3 9.6 %copy-start.32 = (f32[128]{0:T(128)S(1)}, f32[128]{0:T(128)}, u32[]{:S(2)}) copy-start(f32[128]{0:T(128)} %get-tuple-element.155) | copy-start | bytes 1540
  274.3 9.6 %copy-start.33 = (f32[128]{0:T(128)S(1)}, f32[128]{0:T(128)}, u32[]{:S(2)}) copy-start(f32[128]{0:T(128)} %get-tuple-element.156) | copy-start | bytes 1540
  274.3 9.6 %copy-start.34 = (f32[128]{0:T(128)S(1)}, f32[128]{0:T(128)}, u32[]{:S(2)}) copy-start(f32[128]{0:T(128)} %get-tuple-element.157) | copy-start | bytes 1540
  274.3 16.4 %copy-start.1 = (f32[1,128,256]{2,1,0:T(8,128)S(1)}, f32[1,128,256]{2,1,0:T(8,128)}, u32[]{:S(2)}) copy-start(f32[1,128,256]{2,1,0:T(8,128)} %fusion.53) | copy-start | bytes 393220
  277.8 42.2 %copy-start.8 = (f32[16,1,64,256]{3,2,1,0:T(8,128)S(1)}, f32[16,1,64,256]{3,2,1,0:T(8,128)}, u32[]{:S(2)}) copy-start(f32[16,1,64,256]{3,2,1,0:T(8,128)} %get-tuple-element.53) | copy-start | bytes 3145732
  277.9 43.4 %copy-start.5 = (bf16[2048,128]{1,0:T(8,128)(2,1)S(1)}, bf16[2048,128]{1,0:T(8,128)(2,1)}, u32[]{:S(2)}) copy-start(bf16[2048,128]{1,0:T(8,128)(2,1)} %param.23) | copy-start | bytes 1572868
  277.9 43.4 %copy-start.37 = (f32[128]{0:T(128)S(1)}, f32[128]{0:T(128)}, u32[]{:S(2)}) copy-start(f32[128]{0:T(128)} %param.30) | copy-start | bytes 1540
  277.9 5.9 %collective-permute-start = (bf16[30,128]{1,0:T(8,128)(2,1)S(1)}, bf16[30,128]{1,0:T(8,128)(2,1)S(1)}, u32[]{:S(2)}, u32[]{:S(2)}) collective-permute-start(bf16[30,128]{1,0:T(8,128)(2,1)S(1)} %slice.504), channel_id=1, source_target_pairs={{0,8},{8,16},{16,24},{24,32},{32,40},{40,48},{48,56},{56,64},{64,7... | collective-permute-start | bytes 23048 | tf_op jit(solution)/shard_map/ppermute | solution.py:43
  287.3 8.9 %all-to-all-start.1 = ((f32[8,1,2048]{2,1,0:T(1,128)}), f32[8,1,2048]{2,1,0:T(1,128)S(1)}, u32[]{:S(2)}, u32[]{:S(2)}) async-start(f32[8,1,2048]{2,1,0:T(1,128)} %broadcast_in_dim.36), calls=%async_computation.1 | async-start | bytes 131072 | tf_op jit(solution)/shard_map/all_to_all | solution.py:48
  290.7 90.7 %reduce-scatter.2.cloned.1.call-start = ((), (), s32[]{:S(2)}) async-start(), calls=%async_computation.3 | async-start | bytes 4718592 | tf_op jit(solution)/shard_map/reduce_scatter | solution.py:227
  321.3 10.0 %copy-start.3 = (bf16[128,2048]{1,0:T(8,128)(2,1)S(1)}, bf16[128,2048]{1,0:T(8,128)(2,1)}, u32[]{:S(2)}) copy-start(bf16[128,2048]{1,0:T(8,128)(2,1)} %param.35) | copy-start | bytes 1572868
  321.3 10.0 %copy-start.4 = (bf16[2048,128]{1,0:T(8,128)(2,1)S(1)}, bf16[2048,128]{1,0:T(8,128)(2,1)}, u32[]{:S(2)}) copy-start(bf16[2048,128]{1,0:T(8,128)(2,1)} %param.26) | copy-start | bytes 1572868
  321.3 10.0 %copy-start.35 = (f32[128]{0:T(128)S(1)}, f32[128]{0:T(128)}, u32[]{:S(2)}) copy-start(f32[128]{0:T(128)} %param.33) | copy-start | bytes 1540
  321.4 10.0 %copy-start.36 = (f32[128]{0:T(128)S(1)}, f32[128]{0:T(128)}, u32[]{:S(2)}) copy-start(f32[128]{0:T(128)} %param.32) | copy-start | bytes 1540
Sparse Core Ops, SparseCore 0:
  270.6 39.5 all-gather.3
  342.4 38.9 reduce-scatter.1
